TPU v7x, 32 devices: a whole 2x2x4 slice. The times are simulated.
32 devices in a mesh: kv: 4 (over y, x), tp: 8 (over z, core).
Axes of the slice: x: 2, y: 2, z: 4, core: 2. Of those that a mesh axis runs over, the one named last changes fastest.
Arguments:
- tokens: bfloat16 [3, 4096], P(None, ('kv', 'tp')), may hold values from -40 to 40
- lengths: int32 [3], replicated, may hold values from 1 to 8192, as said below
- attn_gain: float32 [4096], P(('kv', 'tp')), may hold values from 0.1 to 1.9
- w_query: bfloat16 [4096, 2048], P('kv', 'tp'), may hold values from -0.09375 to 0.09375
- w_key: bfloat16 [4096, 128], P('kv'), may hold values from -0.09375 to 0.09375
- w_value: bfloat16 [4096, 128], P('kv'), may hold values from -0.09375 to 0.09375
- w_forget: bfloat16 [4096, 32], replicated, may hold values from -0.09375 to 0.09375
- forget_bias: float32 [32], replicated, may hold values from -4 to 0
- cache_keys: bfloat16 [3, 128, 8192], P(None, None, ('kv', 'tp')), may hold values from -320 to 320
- cache_values: bfloat16 [3, 128, 8192], P(None, None, ('kv', 'tp')), may hold values from -6 to 6
- cache_decay: float32 [3, 32, 8192], P(None, None, ('kv', 'tp')), may hold values from -1028 to 0, as said below
- out_gain: float32 [2048], replicated, may hold values from 0.1 to 1.9
- w_out: bfloat16 [2048, 4096], P('tp', 'kv'), may hold values from -0.125 to 0.125
- mlp_gain: float32 [4096], P(('kv', 'tp')), may hold values from 0.1 to 1.9
- w_gate: bfloat16 [4096, 11264], P('kv', 'tp'), may hold values from -0.09375 to 0.09375
- w_up: bfloat16 [4096, 11264], P('kv', 'tp'), may hold values from -0.09375 to 0.09375
- w_down: bfloat16 [11264, 4096], P('tp', 'kv'), may hold values from -0.0546875 to 0.0546875
Outputs:
- layer_out: bfloat16 [3, 4096], P(None, ('kv', 'tp'))
Inputs may be any that keep to these rules, and one draw needn't show every extreme that they name: Sequence b has lengths[b] live cache positions, 0 to lengths[b] - 1; some sequence has exactly 8192 in every draw. On live positions, cache_decay[b, h, j] is the sum of the log forget gates of sequence b and head h over positions j + 1 to lengths[b] - 1, so it is zero at the last live position and never rises toward earlier positions; it is zero beyond lengths[b].
All inputs are finite; a program needn't handle non-finite values.
Results may differ from a plain program's by a relative error of at most 0.013.
Values may be sent and summed in bfloat16 or wider, within the bound.
A program may use at most 64 MiB of HBM per device.

v0:
```python
import jax
import jax.numpy as jnp
from jax import lax
from jax.sharding import PartitionSpec as P

QUERY_HEAD_COUNT = 32
HD = 64
KV_HEADS = 2
epsilon = 1e-06
masked_score = -1e30


def spread_rows(share, gain):
    scaled = (share.astype(jnp.float32) * gain).astype(jnp.bfloat16)
    squares = jnp.sum(jnp.square(share.astype(jnp.float32)), axis=1)
    row_block = lax.all_gather(scaled, "tp", axis=1, tiled=True)
    square_total = lax.psum(squares, ("kv", "tp"))
    return (row_block, square_total)


def body(
    tokens,
    lengths,
    attn_gain,
    w_query,
    w_key,
    w_value,
    w_forget,
    forget_bias,
    cache_keys,
    cache_values,
    cache_decay,
    out_gain,
    w_out,
    mlp_gain,
    w_gate,
    w_up,
    w_down,
):
    full_width = tokens.shape[1] * lax.axis_size("kv") * lax.axis_size("tp")
    kv_index = lax.axis_index("kv")
    tp_index = lax.axis_index("tp")
    row_block, square_total = spread_rows(tokens, attn_gain)
    block_rows = row_block.shape[1]
    forget_rows = lax.dynamic_slice_in_dim(w_forget, kv_index * block_rows, block_rows, 0)
    query_part = jnp.dot(row_block, w_query, preferred_element_type=jnp.float32)
    key_part = jnp.dot(row_block, w_key, preferred_element_type=jnp.float32)
    value_part = jnp.dot(row_block, w_value, preferred_element_type=jnp.float32)
    forget_part = jnp.dot(row_block, forget_rows, preferred_element_type=jnp.float32)
    query_sum, key_sum, value_sum, forget_sum = lax.psum(
        (query_part, key_part, value_part, forget_part), "kv"
    )
    first_rms = lax.rsqrt(square_total / full_width + epsilon)[:, None]
    query_local = (query_sum * first_rms).astype(jnp.bfloat16)
    key_new = (key_sum * first_rms).astype(jnp.bfloat16)
    value_new = (value_sum * first_rms).astype(jnp.bfloat16)
    log_gate = jax.nn.log_sigmoid(forget_sum * first_rms + forget_bias)
    query_all = lax.all_gather(query_local, "tp", axis=1, tiled=True)
    batch_rows, key_dims, span = cache_keys.shape
    groups = QUERY_HEAD_COUNT // KV_HEADS
    score_scale = HD ** (-0.5)
    query_grouped = query_all.reshape(batch_rows, KV_HEADS, groups, HD)
    keys_grouped = cache_keys.reshape(batch_rows, KV_HEADS, HD, span)
    values_grouped = cache_values.reshape(batch_rows, KV_HEADS, HD, span)
    scores = jnp.einsum(
        "bkgd,bkdj->bkgj", query_grouped, keys_grouped, preferred_element_type=jnp.float32
    ).reshape(batch_rows, QUERY_HEAD_COUNT, span)
    scores = scores * score_scale + cache_decay + log_gate[:, :, None]
    first_slot = (kv_index * lax.axis_size("tp") + tp_index) * span
    token_positions = first_slot + lax.iota(jnp.int32, span)
    is_live = (token_positions[None, :] < lengths[:, None])[:, None, :]
    scores = jnp.where(is_live, scores, masked_score)
    own_score = (
        jnp.einsum(
            "inpo,ino->inp",
            query_grouped,
            key_new.reshape(batch_rows, KV_HEADS, HD),
            preferred_element_type=jnp.float32,
        ).reshape(batch_rows, QUERY_HEAD_COUNT)
        * score_scale
    )
    local_top = jnp.maximum(jnp.max(scores, axis=2), own_score)
    head_count = w_out.shape[0] // HD
    head_start = tp_index * head_count
    score_top = lax.pmax(local_top, ("kv", "tp"))
    weights = jnp.where(is_live, jnp.exp(scores - score_top[:, :, None]), 0.0)
    weight_total = jnp.sum(weights, axis=2)
    rounded = weights.astype(jnp.bfloat16).reshape(batch_rows, KV_HEADS, groups, span)
    value_sums = jnp.einsum(
        "bkgj,bkdj->bkgd", rounded, values_grouped, preferred_element_type=jnp.float32
    ).reshape(batch_rows, QUERY_HEAD_COUNT, HD)
    weight_total, value_sums = (weight_total, value_sums)
    weight_total, value_sums = (
        lax.psum_scatter(weight_total, "tp", scatter_dimension=1, tiled=True),
        lax.psum_scatter(value_sums, "tp", scatter_dimension=1, tiled=True),
    )
    weight_total, value_sums = lax.psum((weight_total, value_sums), "kv")
    score_top = lax.dynamic_slice_in_dim(score_top, head_start, head_count, 1)
    own_here = lax.dynamic_slice_in_dim(own_score, head_start, head_count, 1)
    new_values = jnp.repeat(value_new.reshape(batch_rows, KV_HEADS, HD), groups, axis=1)
    new_values = lax.dynamic_slice_in_dim(new_values, head_start, head_count, 1).astype(jnp.float32)
    own_weight = jnp.exp(own_here - score_top)
    heads_out = (value_sums + own_weight[:, :, None] * new_values) / (weight_total + own_weight)[
        :, :, None
    ]
    head_gains = lax.dynamic_slice_in_dim(out_gain, head_start * HD, head_count * HD, 0).reshape(
        head_count, HD
    )
    normed = (
        heads_out
        * lax.rsqrt(jnp.mean(jnp.square(heads_out), axis=2, keepdims=True) + epsilon)
        * head_gains
    )
    normed = normed.astype(jnp.bfloat16).reshape(batch_rows, head_count * HD)
    attn_part = jnp.dot(normed, w_out, preferred_element_type=jnp.float32)
    attn_share = lax.psum_scatter(attn_part, "tp", scatter_dimension=1, tiled=True)
    residual = (tokens.astype(jnp.float32) + attn_share).astype(jnp.bfloat16)
    mlp_block, mlp_squares = spread_rows(residual, mlp_gain)
    gate_part = jnp.dot(mlp_block, w_gate, preferred_element_type=jnp.float32)
    up_part = jnp.dot(mlp_block, w_up, preferred_element_type=jnp.float32)
    gate_sum, up_sum = lax.psum((gate_part, up_part), "kv")
    second_rms = lax.rsqrt(mlp_squares / full_width + epsilon)[:, None]
    hidden = (jax.nn.silu(gate_sum * second_rms) * (up_sum * second_rms)).astype(jnp.bfloat16)
    down_part = jnp.dot(hidden, w_down, preferred_element_type=jnp.float32)
    mlp_share = lax.psum_scatter(down_part, "tp", scatter_dimension=1, tiled=True)
    return (residual.astype(jnp.float32) + mlp_share).astype(jnp.bfloat16)


def solution(mesh):
    placed = (
        P(None, ("kv", "tp")),
        P(),
        P(("kv", "tp")),
        P("kv", "tp"),
        P("kv", None),
        P("kv", None),
        P(),
        P(),
        P(None, None, ("kv", "tp")),
        P(None, None, ("kv", "tp")),
        P(None, None, ("kv", "tp")),
        P(),
        P("tp", "kv"),
        P(("kv", "tp")),
        P("kv", "tp"),
        P("kv", "tp"),
        P("tp", "kv"),
    )
    return jax.shard_map(
        body, mesh=mesh, in_specs=placed, out_specs=P(None, ("kv", "tp")), check_vma=False
    )
```

profile of v0, /device:TPU:0, one launch (start us, length us, event | category | flops | bytes accessed | tf_op | source)
XLA Modules:
  0.0 321.7 jit_solution(4829693310829404246)
XLA Ops:
  6.5 0.9 dynamic_slice.19
  8.9 42.0 %psum.71 = f32[3]{0:T(128)S(1)} all-reduce(f32[3]{0:T(128)S(1)} %get-tuple-element.23), channel_id=1, replica_groups=mesh['kv'=4,'tp'=8] {'kv','tp'}, use_global_device_ids=true, to_apply=%region_2.0 | all-reduce | flops 3 | bytes 24 | tf_op jit(solution)/shard_map/psum | solution.py:17
  51.0 10.6 %all_gather.9 = bf16[3,1024]{1,0:T(4,128)(2,1)S(1)} all-gather(bf16[3,128]{1,0:T(4,128)(2,1)S(1)} %get-tuple-element.24), channel_id=1, replica_groups=mesh['kv'=4,'tp'=8] {'tp'}, dimensions={1}, use_global_device_ids=true | all-gather | bytes 6912 | tf_op jit(solution)/shard_map/all_gather | solution.py:16
  61.5 1.7 fusion.25
  63.2 1.1 fusion.22
  64.3 1.2 fusion.21
  65.5 1.0 fusion.3
  66.5 9.9 %all-reduce.5 = (f32[3,256]{1,0:T(4,128)S(1)}, f32[3,32]{1,0:T(4,128)S(1)}, f32[3,128]{1,0:T(4,128)S(1)}) all-reduce(f32[3,256]{1,0:T(4,128)S(1)} %fusion.21, f32[3,32]{1,0:T(4,128)S(1)} %fusion.3, f32[3,128]{1,0:T(4,128)S(1)} %fusion.22), channel_id=1, replica_groups=mesh['kv'=4,'tp'=8] {'kv'}, use_global_device_ids=true, to_apply=%region_0.0 | all-reduce | flops 1248 | bytes 9984 | tf_op jit(solution)/shard_map/psum | solution.py:50
  76.6 12.8 %all_gather.10 = bf16[3,2048]{1,0:T(4,128)(2,1)S(1)} all-gather(bf16[3,256]{1,0:T(4,128)(2,1)S(1)} %multiply_convert_fusion.1), channel_id=1, replica_groups=mesh['kv'=4,'tp'=8] {'tp'}, dimensions={1}, use_global_device_ids=true | all-gather | bytes 13824 | tf_op jit(solution)/shard_map/all_gather | solution.py:58
  89.7 1.1 convolution_multiply_fusion
  92.2 1.0 fusion
  93.4 37.8 %pmax.7 = f32[3,32]{1,0:T(4,128)} all-reduce(f32[3,32]{1,0:T(4,128)S(1)} %max.17), channel_id=1, replica_groups=mesh['kv'=4,'tp'=8] {'kv','tp'}, use_global_device_ids=true, to_apply=%region_6.7 | all-reduce | flops 96 | bytes 768 | tf_op jit(solution)/shard_map/pmax | solution.py:85
  131.2 1.4 fusion.1
  132.6 1.2 dynamic-slice
  134.5 1.1 fusion.24
  135.6 27.4 %all-reduce.2 = (f32[3,32,64]{2,1,0:T(8,128)S(1)}, f32[3,32]{1,0:T(4,128)S(1)}) all-reduce(f32[3,32,64]{2,1,0:T(8,128)S(1)} %bitcast.42, f32[3,32]{1,0:T(4,128)} %get-tuple-element.21), channel_id=2, replica_groups=mesh['kv'=4,'tp'=8] {'tp'}, use_global_device_ids=true, to_apply=%region_7.8.clone | all-reduce | flops 6240 | bytes 49920
  163.1 16.6 %all-reduce.4 = (f32[3,4,64]{2,1,0:T(4,128)S(1)}, f32[3,4]{1,0:T(4,128)S(1)}, f32[3,128]{1,0:T(4,128)S(1)}) all-reduce(f32[3,4,64]{2,1,0:T(4,128)S(1)} %constant_dynamic-slice_fusion.1, f32[3,4]{1,0:T(4,128)S(1)} %constant_dynamic-slice_fusion, f32[3,128]{1,0:T(4,128)} %fusion.25), channel_id=1, replica_groups=mesh['kv'=4,'tp'=8] {'kv'}, use_global_device_ids=true, to_apply=%region_8.9 | all-reduce | flops 1164 | bytes 9312 | tf_op jit(solution)/shard_map/psum | solution.py:97
  182.3 1.1 convolution_bitcast_fusion.1
  183.5 27.8 %reduce-scatter.9.cloned.1.call-done = f32[128,3]{1,0:T(8,128)} async-done(((f32[1024,3]{1,0:T(8,128)}), f32[128,3]{1,0:T(8,128)}) %reduce-scatter.9.cloned.1.call-update) | async-done | bytes 1552
  213.0 37.8 %psum.78 = f32[3]{0:T(128)S(1)} all-reduce(f32[3]{0:T(128)S(1)} %get-tuple-element.15), channel_id=1, replica_groups=mesh['kv'=4,'tp'=8] {'kv','tp'}, use_global_device_ids=true, to_apply=%region_17.18 | all-reduce | flops 3 | bytes 24 | tf_op jit(solution)/shard_map/psum | solution.py:17
  251.6 11.4 %all_gather.11 = bf16[3,1024]{1,0:T(4,128)(2,1)S(1)} all-gather(bf16[3,128]{1,0:T(4,128)(2,1)S(1)} %fusion.13), channel_id=1, replica_groups=mesh['kv'=4,'tp'=8] {'tp'}, dimensions={1}, use_global_device_ids=true | all-gather | bytes 6912 | tf_op jit(solution)/shard_map/all_gather | solution.py:16
  264.0 16.7 %all-reduce.3 = (f32[3,1408]{1,0:T(4,128)S(1)}, f32[3,1408]{1,0:T(4,128)S(1)}) all-reduce(f32[3,1408]{1,0:T(4,128)S(1)} %fusion.27, f32[3,1408]{1,0:T(4,128)S(1)} %fusion.26), channel_id=1, replica_groups=mesh['kv'=4,'tp'=8] {'kv'}, use_global_device_ids=true, to_apply=%region_18.19 | all-reduce | flops 8448 | bytes 67584 | tf_op jit(solution)/shard_map/psum | solution.py:121
  280.7 3.8 %convolution_bitcast_fusion = f32[1024,3]{1,0:T(8,128)} fusion(bf16[1408,1024]{1,0:T(8,128)(2,1)} %param.33, f32[3,1408]{1,0:T(4,128)S(1)} %get-tuple-element.7, f32[3,1408]{1,0:T(4,128)S(1)} %get-tuple-element.8, f32[3]{0:T(128)S(1)} %add_rsqrt_fusion.1), kind=kOutput, calls=%fused_computation | convolution fusion | flops 8684544 | bytes 2929676
  284.5 28.8 %reduce-scatter.11.cloned.1.call-done = f32[128,3]{1,0:T(8,128)} async-done(((f32[1024,3]{1,0:T(8,128)}), f32[128,3]{1,0:T(8,128)}) %reduce-scatter.11.cloned.1.call-update) | async-done | bytes 1552
  (49 shorter events, 11.3 us)
Async XLA Ops:
  6.5 256.5 %copy-start = (bf16[1024,1408]{1,0:T(8,128)(2,1)S(1)}, bf16[1024,1408]{1,0:T(8,128)(2,1)}, u32[]{:S(2)}) copy-start(bf16[1024,1408]{1,0:T(8,128)(2,1)} %param.32) | copy-start | bytes 8650756
  6.5 175.7 %copy-start.2 = (bf16[256,1024]{1,0:T(8,128)(2,1)S(1)}, bf16[256,1024]{1,0:T(8,128)(2,1)}, u32[]{:S(2)}) copy-start(bf16[256,1024]{1,0:T(8,128)(2,1)} %param.29) | copy-start | bytes 1572868
  6.5 204.8 %reduce-scatter.9.cloned.1.call-start = ((), (), s32[]{:S(2)}) async-start(), calls=%async_computation.2 | async-start | bytes 589824
  50.9 40.6 %copy-start.5 = (f32[3]{0:T(128)}, f32[3]{0:T(128)S(1)}, u32[]{:S(2)}) copy-start(f32[3]{0:T(128)S(1)} %add_rsqrt_fusion.2) | copy-start | bytes 40
  89.7 3.7 %copy-start.3 = (f32[3,32]{1,0:T(4,128)}, f32[3,32]{1,0:T(4,128)S(1)}, u32[]{:S(2)}) copy-start(f32[3,32]{1,0:T(4,128)S(1)} %mul.142) | copy-start | bytes 1156
  91.5 1.7 copy-start.4
  183.4 129.9 %reduce-scatter.11.cloned.1.call-start = ((), (), s32[]{:S(2)}) async-start(), calls=%async_computation.3 | async-start | bytes 589824
  250.8 12.7 %copy-start.1 = (bf16[1024,1408]{1,0:T(8,128)(2,1)S(1)}, bf16[1024,1408]{1,0:T(8,128)(2,1)}, u32[]{:S(2)}) copy-start(bf16[1024,1408]{1,0:T(8,128)(2,1)} %param.31) | copy-start | bytes 8650756
Sparse Core Ops, SparseCore 0:
  183.5 27.7 reduce-scatter.8
  284.6 28.6 reduce-scatter.10
where the time goes:
time: 323 us; the launch traced here: 322 us
  blocking collectives  223 us (69%)
  waiting for transfers between devices  56.7 us (18%)
  between operations  14.1 us (4%)
  matrix products  13.2 us (4%)
  other arithmetic  9.52 us (3%)
  local copies, waits for them, and re-layouts  5.19 us (2%)
    psum x2, blocking collectives, spread_rows(): square_total = lax.psum(squares, ('kv', 'tp'))  79.8 us
    unnamed x4, waiting for transfers between devices  56.7 us
    pmax x1, blocking collectives, body(): score_top = lax.pmax(local_top, ('kv', 'tp'))  37.8 us
    unnamed x1, blocking collectives  27.4 us
    all_gather x2, blocking collectives, spread_rows(): row_block = lax.all_gather(scaled, 'tp', axis=1, tiled=True)  22 us
    psum x1, blocking collectives, body(): gate_sum, up_sum = lax.psum((gate_part, up_part), 'kv')  16.7 us
    psum x1, blocking collectives, body(): weight_total, value_sums = lax.psum((weight_total, value_sums), 'kv')  16.6 us
    all_gather x1, blocking collectives, body(): query_all = lax.all_gather(query_local, 'tp', axis=1, tiled=True)  12.8 us
  transfers between devices with their start and end apart: 2, of which 2 were waited for; matrix products, arithmetic and copies ran while one was open for 0% of the time, Pallas kernels for 0%

commit v1 on v0

--- a/solution.py
+++ b/solution.py
@@ -14,7 +14,7 @@
     scaled = (share.astype(jnp.float32) * gain).astype(jnp.bfloat16)
     squares = jnp.sum(jnp.square(share.astype(jnp.float32)), axis=1)
     row_block = lax.all_gather(scaled, "tp", axis=1, tiled=True)
-    square_total = lax.psum(squares, ("kv", "tp"))
+    square_total = lax.psum(lax.psum(squares, "tp"), "kv")
     return (row_block, square_total)
 
 

time: 323 us -> 271 us (0.84)
  blocking collectives: 223 us -> 170 us
    psum x2, blocking collectives: 79.8 us -> 31.9 us  [spread_rows(): square_total = lax.psum(lax.psum(squares, 'tp'), 'kv')]
    all_gather x2, blocking collectives: 22 us -> 17 us  [spread_rows(): row_block = lax.all_gather(scaled, 'tp', axis=1, tiled=True)]
where the time goes in v1:
time: 271 us; the launch traced here: 270 us
  blocking collectives  170 us (63%)
  waiting for transfers between devices  57 us (21%)
  between operations  14.2 us (5%)
  matrix products  13.2 us (5%)
  other arithmetic  9.51 us (4%)
  local copies, waits for them, and re-layouts  5.19 us (2%)
    unnamed x4, waiting for transfers between devices  57 us
    pmax x1, blocking collectives, body(): score_top = lax.pmax(local_top, ('kv', 'tp'))  38.2 us
    psum x2, blocking collectives, spread_rows(): square_total = lax.psum(lax.psum(squares, 'tp'), 'kv')  31.9 us
    unnamed x1, blocking collectives  27 us
    all_gather x2, blocking collectives, spread_rows(): row_block = lax.all_gather(scaled, 'tp', axis=1, tiled=True)  17 us
    psum x1, blocking collectives, body(): gate_sum, up_sum = lax.psum((gate_part, up_part), 'kv')  16.8 us
    psum x1, blocking collectives, body(): weight_total, value_sums = lax.psum((weight_total, value_sums), 'kv')  16.5 us
    all_gather x1, blocking collectives, body(): query_all = lax.all_gather(query_local, 'tp', axis=1, tiled=True)  12.8 us
  transfers between devices with their start and end apart: 2, of which 2 were waited for; matrix products, arithmetic and copies ran while one was open for 0% of the time, Pallas kernels for 0%

profile of v1, /device:TPU:0, one launch (start us, length us, event | category | flops | bytes accessed | tf_op | source)
XLA Modules:
  0.0 269.6 jit_solution(2129917216340552273)
XLA Ops:
  6.5 0.9 dynamic_slice.19
  8.9 18.1 %psum.85 = f32[3]{0:T(128)S(1)} all-reduce(f32[3]{0:T(128)S(1)} %get-tuple-element.25), channel_id=1, replica_groups=mesh['kv'=4,'tp'=8] {'tp'}, use_global_device_ids=true, to_apply=%region_2.0 | all-reduce | flops 3 | bytes 24 | tf_op jit(solution)/shard_map/psum | solution.py:17
  27.0 8.4 %all_gather.9 = bf16[3,1024]{1,0:T(4,128)(2,1)S(1)} all-gather(bf16[3,128]{1,0:T(4,128)(2,1)S(1)} %get-tuple-element.26), channel_id=1, replica_groups=mesh['kv'=4,'tp'=8] {'tp'}, dimensions={1}, use_global_device_ids=true | all-gather | bytes 6912 | tf_op jit(solution)/shard_map/all_gather | solution.py:16
  35.5 1.7 fusion.25
  37.1 1.1 fusion.22
  38.2 1.2 fusion.21
  39.4 1.0 fusion.3
  40.4 10.2 %all-reduce.5 = (f32[3,256]{1,0:T(4,128)S(1)}, f32[3]{0:T(128)S(1)}, f32[3,32]{1,0:T(4,128)S(1)}, f32[3,128]{1,0:T(4,128)S(1)}) all-reduce(f32[3,256]{1,0:T(4,128)S(1)} %fusion.21, f32[3]{0:T(128)S(1)} %psum.85, f32[3,32]{1,0:T(4,128)S(1)} %fusion.3, f32[3,128]{1,0:T(4,128)S(1)} %fusion.22), channel_id=1, replica_groups=mesh['kv'=4,'tp'=8] {'kv'}, use_global_device_ids=true, to_apply=%region_0.0 | all-reduce | flops 1251 | bytes 10008 | tf_op jit(solution)/shard_map/psum | solution.py:50
  50.9 12.8 %all_gather.10 = bf16[3,2048]{1,0:T(4,128)(2,1)S(1)} all-gather(bf16[3,256]{1,0:T(4,128)(2,1)S(1)} %multiply_convert_fusion.1), channel_id=1, replica_groups=mesh['kv'=4,'tp'=8] {'tp'}, dimensions={1}, use_global_device_ids=true | all-gather | bytes 13824 | tf_op jit(solution)/shard_map/all_gather | solution.py:58
  64.0 1.1 convolution_multiply_fusion
  66.5 1.0 fusion
  67.6 38.2 %pmax.7 = f32[3,32]{1,0:T(4,128)} all-reduce(f32[3,32]{1,0:T(4,128)S(1)} %max.17), channel_id=1, replica_groups=mesh['kv'=4,'tp'=8] {'kv','tp'}, use_global_device_ids=true, to_apply=%region_7.8 | all-reduce | flops 96 | bytes 768 | tf_op jit(solution)/shard_map/pmax | solution.py:85
  105.9 1.4 fusion.1
  107.3 1.2 dynamic-slice
  109.2 1.1 fusion.24
  110.3 27.0 %all-reduce.2 = (f32[3,32,64]{2,1,0:T(8,128)S(1)}, f32[3,32]{1,0:T(4,128)S(1)}) all-reduce(f32[3,32,64]{2,1,0:T(8,128)S(1)} %bitcast.42, f32[3,32]{1,0:T(4,128)} %get-tuple-element.23), channel_id=2, replica_groups=mesh['kv'=4,'tp'=8] {'tp'}, use_global_device_ids=true, to_apply=%region_8.9.clone | all-reduce | flops 6240 | bytes 49920
  137.4 16.5 %all-reduce.4 = (f32[3,4,64]{2,1,0:T(4,128)S(1)}, f32[3,4]{1,0:T(4,128)S(1)}, f32[3,128]{1,0:T(4,128)S(1)}) all-reduce(f32[3,4,64]{2,1,0:T(4,128)S(1)} %constant_dynamic-slice_fusion.1, f32[3,4]{1,0:T(4,128)S(1)} %constant_dynamic-slice_fusion, f32[3,128]{1,0:T(4,128)} %fusion.25), channel_id=1, replica_groups=mesh['kv'=4,'tp'=8] {'kv'}, use_global_device_ids=true, to_apply=%region_9.10 | all-reduce | flops 1164 | bytes 9312 | tf_op jit(solution)/shard_map/psum | solution.py:97
  156.5 1.1 convolution_bitcast_fusion.1
  157.7 27.7 %reduce-scatter.9.cloned.1.call-done = f32[128,3]{1,0:T(8,128)} async-done(((f32[1024,3]{1,0:T(8,128)}), f32[128,3]{1,0:T(8,128)}) %reduce-scatter.9.cloned.1.call-update) | async-done | bytes 1552
  187.1 13.8 %psum.93 = f32[3]{0:T(128)S(1)} all-reduce(f32[3]{0:T(128)S(1)} %get-tuple-element.17), channel_id=1, replica_groups=mesh['kv'=4,'tp'=8] {'tp'}, use_global_device_ids=true, to_apply=%region_18.19 | all-reduce | flops 3 | bytes 24 | tf_op jit(solution)/shard_map/psum | solution.py:17
  201.7 8.6 %all_gather.11 = bf16[3,1024]{1,0:T(4,128)(2,1)S(1)} all-gather(bf16[3,128]{1,0:T(4,128)(2,1)S(1)} %fusion.13), channel_id=1, replica_groups=mesh['kv'=4,'tp'=8] {'tp'}, dimensions={1}, use_global_device_ids=true | all-gather | bytes 6912 | tf_op jit(solution)/shard_map/all_gather | solution.py:16
  211.3 16.8 %all-reduce.3 = (f32[3,1408]{1,0:T(4,128)S(1)}, f32[3,1408]{1,0:T(4,128)S(1)}, f32[3]{0:T(128)S(1)}) all-reduce(f32[3,1408]{1,0:T(4,128)S(1)} %fusion.27, f32[3,1408]{1,0:T(4,128)S(1)} %fusion.26, f32[3]{0:T(128)S(1)} %psum.93), channel_id=1, replica_groups=mesh['kv'=4,'tp'=8] {'kv'}, use_global_device_ids=true, to_apply=%region_20.21 | all-reduce | flops 8451 | bytes 67608 | tf_op jit(solution)/shard_map/psum | solution.py:121
  228.1 3.8 %convolution_bitcast_fusion = f32[1024,3]{1,0:T(8,128)} fusion(bf16[1408,1024]{1,0:T(8,128)(2,1)} %param.33, f32[3,1408]{1,0:T(4,128)S(1)} %get-tuple-element.7, f32[3,1408]{1,0:T(4,128)S(1)} %get-tuple-element.8, f32[3]{0:T(128)S(1)} %add_rsqrt_fusion.1), kind=kOutput, calls=%fused_computation | convolution fusion | flops 8684544 | bytes 2929676
  232.0 29.3 %reduce-scatter.11.cloned.1.call-done = f32[128,3]{1,0:T(8,128)} async-done(((f32[1024,3]{1,0:T(8,128)}), f32[128,3]{1,0:T(8,128)}) %reduce-scatter.11.cloned.1.call-update) | async-done | bytes 1552
  (49 shorter events, 11.3 us)
Async XLA Ops:
  6.5 203.8 %copy-start = (bf16[1024,1408]{1,0:T(8,128)(2,1)S(1)}, bf16[1024,1408]{1,0:T(8,128)(2,1)}, u32[]{:S(2)}) copy-start(bf16[1024,1408]{1,0:T(8,128)(2,1)} %param.32) | copy-start | bytes 8650756
  6.5 149.9 %copy-start.2 = (bf16[256,1024]{1,0:T(8,128)(2,1)S(1)}, bf16[256,1024]{1,0:T(8,128)(2,1)}, u32[]{:S(2)}) copy-start(bf16[256,1024]{1,0:T(8,128)(2,1)} %param.29) | copy-start | bytes 1572868
  6.5 178.8 %reduce-scatter.9.cloned.1.call-start = ((), (), s32[]{:S(2)}) async-start(), calls=%async_computation.2 | async-start | bytes 589824
  50.6 15.1 %copy-start.5 = (f32[3]{0:T(128)}, f32[3]{0:T(128)S(1)}, u32[]{:S(2)}) copy-start(f32[3]{0:T(128)S(1)} %add_rsqrt_fusion.2) | copy-start | bytes 40
  64.0 3.7 %copy-start.3 = (f32[3,32]{1,0:T(4,128)}, f32[3,32]{1,0:T(4,128)S(1)}, u32[]{:S(2)}) copy-start(f32[3,32]{1,0:T(4,128)S(1)} %mul.142) | copy-start | bytes 1156
  65.8 1.7 copy-start.4
  157.6 103.7 %reduce-scatter.11.cloned.1.call-start = ((), (), s32[]{:S(2)}) async-start(), calls=%async_computation.3 | async-start | bytes 589824
  200.9 9.8 %copy-start.1 = (bf16[1024,1408]{1,0:T(8,128)(2,1)S(1)}, bf16[1024,1408]{1,0:T(8,128)(2,1)}, u32[]{:S(2)}) copy-start(bf16[1024,1408]{1,0:T(8,128)(2,1)} %param.31) | copy-start | bytes 8650756
Sparse Core Ops, SparseCore 0:
  157.7 27.5 reduce-scatter.8
  232.1 29.1 reduce-scatter.10
